TPU v7x, 32 devices: a whole 2x2x4 slice. The times are simulated.
32 devices in a mesh: ep: 4 (over y, x), tp: 8 (over z, core).
Axes of the slice: x: 2, y: 2, z: 4, core: 2. Of those that a mesh axis runs over, the one named last changes fastest.
Arguments:
- tokens: bfloat16 [128, 4096], P('ep'), may hold values from -6 to 6
- norm_gain: float32 [4096], replicated, may hold values from 0.1 to 1.9
- group_ids: int32 [128, 1], P('ep'), may hold values from 0 to 1; in each aligned block of 32 rows (0 to 31, 32 to 63, ...) at most 32 rows name the same one
- local_ids: int32 [128, 4], P('ep'), may hold values from 0 to 7, all different within a row
- group_gate: float32 [128], P('ep'), may hold values from 0.3 to 1
- expert_gate: float32 [128, 4], P('ep'), may hold values from 0.1 to 1
- lengths: int32 [32], P('ep'), may hold values from 1 to 4, 64 in all
- w_gate: bfloat16 [16, 1024, 4096], P('ep', 'tp'), may hold values from -0.09375 to 0.09375
- w_up: bfloat16 [16, 1024, 4096], P('ep', 'tp'), may hold values from -0.09375 to 0.09375
- w_down: bfloat16 [16, 1024, 4096], P('ep', None, 'tp'), may hold values from -0.1875 to 0.1875
Outputs:
- mixed: bfloat16 [128, 4096], P('ep', 'tp')
Inputs may be any that keep to these rules, and one draw needn't show every extreme that they name: `group_ids`: among the 32 rows of one index of ep no group is named by more than 32 rows, and some index reaches 32. `local_ids`: each row names 4 different experts of its group. `lengths`: the first that many of a sequence's 4 positions are live.
All inputs are finite; a program needn't handle non-finite values. No bound on the sum of `lengths` on one device may be relied on, other than what follows from the above.
Results may differ from a plain program's by a relative error of at most 0.0065.
Values may be sent and summed in bfloat16 or wider, within the bound.
A program may use at most 64 MiB of HBM per device.

v0:
```python
import jax
import jax.numpy as jnp
from jax import lax
from jax.sharding import PartitionSpec as P

EXP_PER_GROUP = 8
STEP_TOK = 4


def norm_rows(tokens, norm_gain):
    values = tokens.astype(jnp.float32)
    scale = lax.rsqrt(jnp.mean(values * values, axis=1, keepdims=True) + 1e-06)
    return (values * scale * norm_gain).astype(jnp.bfloat16)


def live_mask(lengths, tok_rows):
    places = jnp.arange(tok_rows, dtype=jnp.int32)
    within = places % STEP_TOK
    owner = places // STEP_TOK
    seq_ids = jnp.arange(lengths.shape[0], dtype=jnp.int32)
    hits = (owner[:, None] == seq_ids[None, :]) & (within[:, None] < lengths[None, :])
    return jnp.any(hits, axis=1).astype(jnp.float32)


def expert_hidden(rows, w_gate, w_up):
    gate_part = jnp.einsum("rd,efd->ref", rows, w_gate, preferred_element_type=jnp.float32)
    up_part = jnp.einsum("rd,efd->ref", rows, w_up, preferred_element_type=jnp.float32)
    return (jax.nn.silu(gate_part) * up_part).astype(jnp.bfloat16)


def local(
    tokens, norm_gain, group_ids, local_ids, group_gate, expert_gate, lengths, w_gate, w_up, w_down
):
    highest = lax.Precision.HIGHEST
    tok_rows = tokens.shape[0]
    exp_dev = w_gate.shape[0]
    width_part = w_down.shape[2]
    ep_size = lax.axis_size("ep")
    groups = exp_dev * ep_size // EXP_PER_GROUP
    normed = norm_rows(tokens, norm_gain)
    live = live_mask(lengths, tok_rows)
    local_cols = jnp.arange(EXP_PER_GROUP, dtype=jnp.int32)
    picks = (local_ids[:, :, None] == local_cols[None, None, :]).astype(jnp.float32)
    weights = expert_gate * (group_gate * live)[:, None]
    dense = jnp.sum(picks * weights[:, :, None], axis=1)
    group_cols = jnp.arange(groups, dtype=jnp.int32)
    member_int = (group_ids == group_cols[None, :]).astype(jnp.int32)
    member = member_int.astype(jnp.float32)
    capacity = 2 * tok_rows // groups
    counts = jnp.cumsum(member_int, axis=0)
    rank = jnp.sum((counts - 1) * member_int, axis=1)
    slot_ids = jnp.arange(capacity, dtype=jnp.int32)
    select = member.T[:, None, :] * (rank[None, None, :] == slot_ids[None, :, None]).astype(
        jnp.float32
    )
    rows_by_group = jnp.einsum(
        "gct,td->gcd", select.astype(jnp.bfloat16), normed, preferred_element_type=jnp.float32
    ).astype(jnp.bfloat16)
    gates_by_group = jnp.einsum("gct,tl->gcl", select, dense, precision=highest)
    share = EXP_PER_GROUP // exp_dev
    send_rows = jnp.repeat(rows_by_group, share, axis=0)
    send_gates = gates_by_group.reshape(groups, capacity, share, exp_dev).transpose(0, 2, 1, 3)
    send_gates = send_gates.reshape(ep_size, capacity, exp_dev)
    recv_rows = lax.all_to_all(send_rows, "ep", split_axis=0, concat_axis=0, tiled=True)
    recv_gates = lax.all_to_all(send_gates, "ep", split_axis=0, concat_axis=0, tiled=True)
    slot_rows = recv_rows.reshape(ep_size * capacity, recv_rows.shape[2])
    slot_gates = recv_gates.reshape(ep_size * capacity, exp_dev)
    hidden = expert_hidden(slot_rows, w_gate, w_up)
    total = jnp.einsum(
        "ref,efd->red",
        lax.all_gather(hidden, "tp", axis=2, tiled=True),
        w_down,
        preferred_element_type=jnp.float32,
    )
    results = jnp.einsum("re,red->rd", slot_gates, total, precision=highest)
    results = results.reshape(ep_size, capacity, width_part)
    back = lax.all_to_all(results, "ep", split_axis=0, concat_axis=0, tiled=True)
    grouped = jnp.sum(back.reshape(groups, share, capacity, width_part), axis=1)
    mixed = jnp.einsum("gct,gcd->td", select, grouped, precision=highest)
    return mixed.astype(jnp.bfloat16)


def solution(mesh):
    in_specs = (
        P("ep", None),
        P(),
        P("ep", None),
        P("ep", None),
        P("ep"),
        P("ep", None),
        P("ep"),
        P("ep", "tp", None),
        P("ep", "tp", None),
        P("ep", None, "tp"),
    )
    out_specs = P("ep", "tp")
    return jax.shard_map(local, mesh=mesh, in_specs=in_specs, out_specs=out_specs, check_vma=False)
```

profile of v0, /device:TPU:0, one launch (start us, length us, event | category | flops | bytes accessed | tf_op | source)
XLA Modules:
  0.0 81.1 jit_solution(2347612556403566781)
XLA Ops:
  6.5 0.0 all-gather.2.cloned.1.call-start
  6.5 0.7 fusion.25
  7.2 0.7 fusion.17
  7.9 1.1 %fusion.4 = f32[32]{0:T(128)S(1)} fusion(bf16[32,4096]{1,0:T(8,128)(2,1)} %param.10), kind=kLoop, calls=%fused_computation.10 | loop fusion | flops 393184 | bytes 262272 | tf_op jit(solution)/shard_map/reduce_sum | solution.py:12
  9.0 0.1 reduce_window_sum.11
  9.1 0.0 copy-start
  9.1 1.0 %select_reduce_fusion.1 = s32[32]{0:T(128)S(1)} fusion(s32[32,2]{1,0:T(8,128)S(1)} %reduce_window_sum.11, s32[32]{0:T(128)} %bitcast.46), kind=kLoop, calls=%fused_computation.27 | loop fusion | flops 224 | bytes 512 | tf_op jit(solution)/shard_map/reduce_sum | solution.py:51
  10.1 0.1 fusion.21
  10.2 1.6 %convolution_convert_fusion = bf16[2,32,4096]{2,1,0:T(8,128)(2,1)S(1)} fusion(bf16[32,4096]{1,0:T(8,128)(2,1)} %param.10, f32[4096]{0:T(1024)} %param.11, f32[32]{0:T(128)S(1)} %add_rsqrt_fusion, f32[32,32]{0,1:T(8,128)S(1)} %fusion.21, f32[2,32]{1,0:T(2,128)S(1)} %fusion.25), kind=kOutput, calls=%fused_computation | convolution fusion | flops 17567744 | bytes 807296 | tf_op jit(solution)/shard_map/gct,td->gcd/dot_general | solution.py:56
  11.7 0.1 broadcast_in_dim.2
  11.8 0.0 copy-start.4
  11.8 19.4 %all_to_all.15 = bf16[4,32,4096]{2,1,0:T(8,128)(2,1)S(1)} all-to-all(bf16[4,32,4096]{2,1,0:T(8,128)(2,1)S(1)} %bitcast.37), channel_id=1, replica_groups=mesh['ep'=4,'tp'=8] {'ep'}, dimensions={0} | all-to-all | bytes 2097152 | tf_op jit(solution)/shard_map/all_to_all | solution.py:64
  31.3 0.0 copy-done
  31.3 1.5 %fusion.27 = f32[128,4,128]{2,0,1:T(8,128)S(1)} fusion(bf16[128,4096,1]{1,0,2:T(8,128)(2,1)S(1)} %bitcast.38, bf16[4,128,4096]{2,1,0:T(8,128)(2,1)S(1)} %copy-done), kind=kOutput, calls=%fused_computation.51 | convolution fusion | flops 536870912 | bytes 5505024 | tf_op jit(solution)/shard_map/rd,efd->ref/dot_general | solution.py:26
  32.8 0.0 copy-done.4
  32.8 0.0 copy-start.3
  32.8 0.0 copy-start.5
  32.8 0.0 copy-start.1
  32.8 0.0 copy-start.2
  32.8 2.2 %fusion = bf16[128,4,128]{2,0,1:T(8,128)(2,1)} fusion(bf16[128,4096,1]{1,0,2:T(8,128)(2,1)S(1)} %bitcast.39, bf16[4,128,4096]{2,1,0:T(8,128)(2,1)S(1)} %copy-done.4, f32[128,4,128]{2,0,1:T(8,128)S(1)} %fusion.27), kind=kOutput, calls=%fused_computation.3 | convolution fusion | flops 537264128 | bytes 5636096 | tf_op jit(solution)/shard_map/rd,efd->ref/dot_general | solution.py:27
  35.0 0.0 all-gather.2.cloned.1.call-update
  35.1 0.0 copy-done.3
  35.1 0.1 fusion.24
  35.2 0.0 copy-done.5
  35.2 0.0 copy-done.1
  35.2 0.0 copy-done.2
  35.2 0.2 fusion.12
  35.4 0.1 pad_maximum_fusion
  35.5 0.1 reshape.102
  35.6 0.1 reshape.115
  35.7 7.0 %all_to_all.16 = f32[4,1,128]{2,1,0:T(1,128)S(1)} all-to-all(f32[4,1,128]{2,1,0:T(1,128)S(1)} %reshape.115), channel_id=1, replica_groups=mesh['ep'=4,'tp'=8] {'ep'}, dimensions={0} | all-to-all | bytes 4096 | tf_op jit(solution)/shard_map/all_to_all | solution.py:65
  42.7 0.5 broadcast.120
  43.2 0.7 reduce
  43.9 0.1 reshape.116
  44.0 0.1 copy.43
  44.1 14.7 %all-gather.2.cloned.1.call-done = bf16[128,4,1024]{2,0,1:T(8,128)(2,1)} async-done(((bf16[128,4,128]{2,0,1:T(8,128)(2,1)}), bf16[128,4,1024]{2,0,1:T(8,128)(2,1)}) %all-gather.2.cloned.1.call-update) | async-done | bytes 1048592 | tf_op jit(solution)/shard_map/all_gather | solution.py:71
  58.8 3.2 %convolution_bitcast_fusion = f32[128,4,512]{2,0,1:T(8,128)S(1)} fusion(bf16[128,4,1024]{2,0,1:T(8,128)(2,1)} %all-gather.2.cloned.1.call-done, bf16[4,1024,512]{2,1,0:T(8,128)(2,1)} %param.19), kind=kOutput, calls=%fused_computation.1 | convolution fusion | flops 536870912 | bytes 6291456 | tf_op jit(solution)/shard_map/ref,efd->red/dot_general | solution.py:69
  62.0 2.4 %fusion.2 = f32[128,1,512]{2,1,0:T(1,128)S(1)} fusion(f32[128,4,1]{1,2,0:T(1,128)S(1)} %bitcast.41, f32[128,4,512]{2,0,1:T(8,128)S(1)} %convolution_bitcast_fusion), kind=kOutput, calls=%fused_computation.6 | convolution fusion | flops 3145728 | bytes 1312768 | tf_op jit(solution)/shard_map/re,red->rd/dot_general | solution.py:75
  64.5 8.8 %all_to_all.17 = f32[4,32,512]{2,1,0:T(8,128)S(1)} all-to-all(f32[4,32,512]{2,1,0:T(8,128)S(1)} %bitcast.40), channel_id=1, replica_groups=mesh['ep'=4,'tp'=8] {'ep'}, dimensions={0} | all-to-all | bytes 524288 | tf_op jit(solution)/shard_map/all_to_all | solution.py:77
  73.3 0.9 %fusion.1 = bf16[32,512]{1,0:T(8,128)(2,1)} fusion(f32[2,32,512]{2,1,0:T(8,128)S(1)} %bitcast_reduce_fusion, f32[32,32]{0,1:T(8,128)S(1)} %fusion.21, f32[2,32]{1,0:T(2,128)S(1)} %fusion.25), kind=kOutput, calls=%fused_computation.5 | convolution fusion | flops 12601344 | bytes 168192 | tf_op jit(solution)/shard_map/gct,gcd->td/dot_general | solution.py:79
  (10 shorter events, 0.1 us)
Async XLA Ops:
  6.5 52.3 %all-gather.2.cloned.1.call-start = ((), (), s32[]{:S(2)}) async-start(), calls=%async_computation.3 | async-start | bytes 1179648 | tf_op jit(solution)/shard_map/all_gather | solution.py:71
  9.1 22.2 %copy-start = (bf16[4,128,4096]{2,1,0:T(8,128)(2,1)S(1)}, bf16[4,128,4096]{2,1,0:T(8,128)(2,1)}, u32[]{:S(2)}) copy-start(bf16[4,128,4096]{2,1,0:T(8,128)(2,1)} %param.17) | copy-start | bytes 12582916
  11.8 21.0 %copy-start.4 = (bf16[4,128,4096]{2,1,0:T(8,128)(2,1)S(1)}, bf16[4,128,4096]{2,1,0:T(8,128)(2,1)}, u32[]{:S(2)}) copy-start(bf16[4,128,4096]{2,1,0:T(8,128)(2,1)} %param.18) | copy-start | bytes 12582916
  32.8 2.3 %copy-start.3 = (s32[8]{0:T(128)S(1)}, s32[8]{0:T(128)}, u32[]{:S(2)}) copy-start(s32[8]{0:T(128)} %param.16) | copy-start | bytes 100
  32.8 2.4 %copy-start.5 = (f32[32]{0:T(128)S(1)}, f32[32]{0:T(128)}, u32[]{:S(2)}) copy-start(f32[32]{0:T(128)} %param.14) | copy-start | bytes 388
  32.8 2.4 %copy-start.1 = (f32[32,4]{0,1:T(4,128)S(1)}, f32[32,4]{0,1:T(4,128)}, u32[]{:S(2)}) copy-start(f32[32,4]{0,1:T(4,128)} %param.15) | copy-start | bytes 1540
  32.8 2.4 %copy-start.2 = (s32[32,4]{0,1:T(4,128)S(1)}, s32[32,4]{0,1:T(4,128)}, u32[]{:S(2)}) copy-start(s32[32,4]{0,1:T(4,128)} %param.13) | copy-start | bytes 1540
Sparse Core Ops, SparseCore 0:
  35.2 23.5 all-gather.1
where the time goes:
time: 81.4 us; the launch traced here: 81.1 us
  blocking collectives  35.2 us (43%)
  waiting for transfers between devices  14.7 us (18%)
  between operations  13.6 us (17%)
  matrix products  12.1 us (15%)
  other arithmetic  4.48 us (6%)
  local copies, waits for them, and re-layouts  1.06 us (1%)
    all_to_all x1, blocking collectives, local(): lax.all_to_all(send_rows, 'ep', split_axis=0, concat_axis=0, tiled=True)  19.4 us
    all_gather x1, waiting for transfers between devices, local(): lax.all_gather(hidden, 'tp', axis=2, tiled=True)  14.7 us
    all_to_all x1, blocking collectives, local(): lax.all_to_all(results, 'ep', split_axis=0, concat_axis=0, tiled=True)  8.79 us
    all_to_all x1, blocking collectives, local(): lax.all_to_all(send_gates, 'ep', split_axis=0, concat_axis=0, tiled=True)  7.01 us
    dot_general x1, matrix products, local(): jnp.einsum('ref,efd->red', lax.all_gather(hidden, 'tp', axis=2, tiled=Tru...  3.23 us
    dot_general x1, matrix products, local(): results = jnp.einsum('re,red->rd', slot_gates, total, precision=highest)  2.43 us
    dot_general x1, matrix products, expert_hidden(): jnp.einsum('rd,efd->ref', rows, w_up, preferred_element_type=jnp.float32)  2.18 us
  transfers between devices with their start and end apart: 1, of which 1 were waited for; matrix products, arithmetic and copies ran while one was open for 2% of the time, Pallas kernels for 0%

commit v1 on v0

v1 whole, which is shorter than its diff:
```python
import functools

import jax
import jax.numpy as jnp
from jax import lax
from jax.experimental import pallas as pl
from jax.experimental.pallas import tpu as pltpu
from jax.sharding import PartitionSpec as P

EXP_PER_GROUP = 8
STEP_TOK = 4
CORES = 2
CHUNKS = 4
MESH = pl.DeviceIdType.MESH
F32 = jnp.float32
BF16 = jnp.bfloat16


def token_table(group_ids, local_ids, group_gate, expert_gate, lengths, ep_size, exp_dev):
    top_k, tok_rows = local_ids.shape
    seqs = lengths.shape[1]
    rows = table_rows(exp_dev)
    here = lax.broadcasted_iota(jnp.int32, (seqs, seqs), 0) == lax.broadcasted_iota(jnp.int32, (seqs, seqs), 1)
    column = jnp.sum(jnp.where(here, lengths.astype(F32), 0.0), axis=1, keepdims=True)
    place = lax.broadcasted_iota(jnp.int32, (seqs, tok_rows), 1)
    first = lax.broadcasted_iota(jnp.int32, (seqs, tok_rows), 0) * STEP_TOK
    hits = (place >= first) & (place < first + STEP_TOK) & ((place - first).astype(F32) < column)
    live = jnp.sum(jnp.where(hits, 1.0, 0.0), axis=0, keepdims=True)
    weights = expert_gate * (group_gate * live)
    chosen = group_ids * EXP_PER_GROUP + local_ids
    parts = []
    for owner in range(ep_size):
        row = lax.broadcasted_iota(jnp.int32, (rows, tok_rows), 0)
        part = jnp.where(row == exp_dev, live, 0.0)
        expert = jnp.where(row < exp_dev, owner * exp_dev + row, -1)
        for c in range(top_k):
            part = part + jnp.where(expert == chosen[c:c + 1], weights[c:c + 1], 0.0)
        parts.append(part)
    return parts


def table_rows(exp_dev):
    return -(-(exp_dev + 1) // 8) * 8


def kernel(
    ep_size, tp_size,
    tokens_hbm, gain_ref, group_ref, local_ref, group_gate_ref, expert_gate_ref, lengths_ref, wg_hbm, wu_hbm, wd_hbm,
    out_ref,
    tok, x_all, table_ref, meta, wgu, wd, acc, hid, y_send, y_recv,
    tok_sem, wg_sem, wu_sem, wd_sem,
    meta_send, meta_recv, row_send, row_recv, rowf_send, rowf_recv,
    hid_send, hid_recv, hidp_send, hidp_recv, back_send, back_recv,
):
    exp_dev, part, depth = wg_hbm.shape
    tok_rows = tok.shape[0]
    half = tok_rows // CORES
    n_tok = ep_size * tok_rows
    n_slot = n_tok // 2
    step = depth // CHUNKS
    chips = tp_size // CORES
    ep = lax.axis_index("ep")
    tp = lax.axis_index("tp")
    core = lax.rem(tp, CORES)
    chip = tp // CORES
    partner = chip * CORES + (1 - core)

    def remote(src, dst, send, recv, to_ep, to_tp):
        return pltpu.make_async_remote_copy(
            src_ref=src, dst_ref=dst, send_sem=send, recv_sem=recv,
            device_id=(to_ep, to_tp), device_id_type=MESH,
        )

    def ep_at(off):
        return lax.rem(ep + off + ep_size, ep_size)

    def tp_at(off):
        return lax.rem(chip + off + chips, chips) * CORES + core

    tok_copy = pltpu.make_async_copy(tokens_hbm, tok, tok_sem)
    tok_copy.start()
    wg_copies, wu_copies, wd_copies = [], [], []
    for e in range(exp_dev):
        wg_copies.append(pltpu.make_async_copy(wg_hbm.at[e], wgu.at[e, pl.ds(0, part)], wg_sem.at[e]))
        wu_copies.append(pltpu.make_async_copy(wu_hbm.at[e], wgu.at[e, pl.ds(part, part)], wu_sem.at[e]))
        wd_copies.append(pltpu.make_async_copy(wd_hbm.at[e], wd.at[e], wd_sem.at[e]))
    for copy in wg_copies + wu_copies + wd_copies:
        copy.start()

    barrier = pltpu.get_barrier_semaphore()
    for off in range(1, ep_size):
        pl.semaphore_signal(barrier, inc=1, device_id=(ep_at(off), tp), device_id_type=MESH)
    for off in range(1, chips):
        pl.semaphore_signal(barrier, inc=1, device_id=(ep, tp_at(off)), device_id_type=MESH)
    pl.semaphore_signal(barrier, inc=1, device_id=(ep, partner), device_id_type=MESH)

    tables = token_table(
        group_ref[...], local_ref[...], group_gate_ref[...], expert_gate_ref[...], lengths_ref[...], ep_size, exp_dev
    )
    for i in range(ep_size):
        table_ref[i] = tables[i]
    tok_copy.wait()
    values = tok[...].astype(F32)
    scale = lax.rsqrt(jnp.mean(values * values, axis=1, keepdims=True) + 1e-06)
    x_all[ep] = (values * scale * gain_ref[...]).astype(BF16)
    meta[ep] = table_ref[ep]

    pl.semaphore_wait(barrier, ep_size - 1 + chips - 1 + 1)

    pending = []
    for off in range(1, ep_size):
        copy = remote(table_ref.at[ep_at(off)], meta.at[ep], meta_send.at[off], meta_recv.at[off], ep_at(off), tp)
        copy.start()
        pending.append(copy)

    def rows_of(owner, which, q):
        return x_all.at[owner, pl.ds(pl.multiple_of(which * half, half), half), pl.ds(q * step, step)]

    row_copies = {}
    for q in range(CHUNKS):
        for off in range(1, ep_size):
            block = rows_of(ep, core, q)
            copy = remote(block, block, row_send.at[q, off], row_recv.at[q, off], ep_at(off), tp)
            copy.start()
            row_copies[q, off] = copy
            pending.append(copy)

    for off in range(1, ep_size):
        remote(table_ref.at[ep], meta.at[ep_at(-off)], meta_send.at[off], meta_recv.at[off], ep, tp).wait_recv()
    table = jnp.concatenate([meta[i] for i in range(ep_size)], axis=1)
    live = table[exp_dev:exp_dev + 1, :]
    before = (
        lax.broadcasted_iota(jnp.int32, (n_tok, n_tok), 0) < lax.broadcasted_iota(jnp.int32, (n_tok, n_tok), 1)
    ).astype(F32)
    rank = jnp.dot(
        jnp.broadcast_to(live, (8, n_tok)).astype(BF16), before.astype(BF16), preferred_element_type=F32
    )[0:1, :]
    slot = lax.broadcasted_iota(jnp.int32, (n_tok, n_tok), 0).astype(F32)
    place = jnp.where((slot == rank) & (live > 0.5), 1.0, 0.0)
    pick = place[:n_slot, :]
    spread = jnp.transpose(place)[:, :n_slot].astype(BF16)
    pick16 = pick.astype(BF16)
    gates = [jnp.sum(pick * table[e:e + 1, :], axis=1, keepdims=True) for e in range(exp_dev)]

    def send_hidden(e):
        both = acc[e]
        gate, up = both[:, :part], both[:, part:]
        hid[e, tp] = (jax.nn.silu(gate) * up).astype(BF16)
        block = hid.at[e, tp]
        for off in range(1, chips):
            copy = remote(block, block, hid_send.at[e, off], hid_recv.at[e, off], ep, tp_at(off))
            copy.start()
            pending.append(copy)
        copy = remote(block, block, hidp_send.at[e, 0], hidp_recv.at[e, 0], ep, partner)
        copy.start()
        pending.append(copy)

    for q in range(CHUNKS + 1):
        if q < CHUNKS:
            for off in range(1, ep_size):
                block = rows_of(ep_at(-off), core, q)
                row_copies[q, off].wait_recv()
                copy = remote(block, block, rowf_send.at[q, off], rowf_recv.at[q, off], ep, partner)
                copy.start()
                pending.append(copy)
                row_copies[q, off] = copy
        if q > 0:
            k = q - 1
            for off in range(1, ep_size):
                row_copies[k, off].wait_recv()
            chunk = jnp.concatenate([x_all[i, :, pl.ds(k * step, step)] for i in range(ep_size)], axis=0)
            rows = jnp.dot(pick16, chunk, preferred_element_type=F32).astype(BF16)
            for e in range(exp_dev):
                if k == 0:
                    wg_copies[e].wait()
                    wu_copies[e].wait()
                new = lax.dot_general(
                    rows, wgu[e, :, pl.ds(k * step, step)], (((1,), (1,)), ((), ())), preferred_element_type=F32
                )
                acc[e] = new if k == 0 else acc[e] + new
                if k == CHUNKS - 1:
                    send_hidden(e)

    hid_copies = {}
    total = None
    for e in range(exp_dev + 1):
        if e < exp_dev:
            for off in range(1, chips):
                block = hid.at[e, tp_at(-off)]
                remote(block, block, hid_send.at[e, off], hid_recv.at[e, off], ep, tp_at(off)).wait_recv()
                copy = remote(block, block, hidp_send.at[e, off], hidp_recv.at[e, off], ep, partner)
                copy.start()
                pending.append(copy)
                hid_copies[e, off] = copy
        if e > 0:
            k = e - 1
            block = hid.at[k, tp]
            remote(block, block, hidp_send.at[k, 0], hidp_recv.at[k, 0], ep, partner).wait_recv()
            for off in range(1, chips):
                hid_copies[k, off].wait_recv()
            wd_copies[k].wait()
            hidden = jnp.concatenate([hid[k, j] for j in range(tp_size)], axis=1)
            term = gates[k] * jnp.dot(hidden, wd[k], preferred_element_type=F32)
            total = term if total is None else total + term

    back = jnp.dot(spread, total.astype(BF16), preferred_element_type=F32).astype(BF16)
    for i in range(ep_size):
        y_send[i] = back[i * tok_rows:(i + 1) * tok_rows]
    back_copies = []
    for off in range(1, ep_size):
        copy = remote(y_send.at[ep_at(off)], y_recv.at[off], back_send.at[off], back_recv.at[off], ep_at(off), tp)
        copy.start()
        back_copies.append(copy)
    mixed = y_send[ep].astype(F32)
    for off in range(1, ep_size):
        back_copies[off - 1].wait_recv()
        mixed = mixed + y_recv[off].astype(F32)
    out_ref[...] = mixed.astype(BF16)
    for copy in pending + back_copies:
        copy.wait_send()


def local(
    ep_size, tp_size,
    tokens, norm_gain, group_ids, local_ids, group_gate, expert_gate, lengths, w_gate, w_up, w_down
):
    tok_rows, depth = tokens.shape
    exp_dev, part, _ = w_gate.shape
    _, hidden_all, width = w_down.shape
    chips = tp_size // CORES
    n_slot = ep_size * tok_rows // 2
    rows = table_rows(exp_dev)
    anywhere = pl.BlockSpec(memory_space=pl.ANY)
    vmem = pl.BlockSpec(memory_space=pltpu.VMEM)
    dma = pltpu.SemaphoreType.DMA
    return pl.pallas_call(
        functools.partial(kernel, ep_size, tp_size),
        out_shape=jax.ShapeDtypeStruct((tok_rows, width), BF16),
        in_specs=[anywhere, vmem, vmem, vmem, vmem, vmem, vmem, anywhere, anywhere, anywhere],
        out_specs=vmem,
        scratch_shapes=[
            pltpu.VMEM((tok_rows, depth), BF16),
            pltpu.VMEM((ep_size, tok_rows, depth), BF16),
            pltpu.VMEM((ep_size, rows, tok_rows), F32),
            pltpu.VMEM((ep_size, rows, tok_rows), F32),
            pltpu.VMEM((exp_dev, 2 * part, depth), BF16),
            pltpu.VMEM((exp_dev, hidden_all, width), BF16),
            pltpu.VMEM((exp_dev, n_slot, 2 * part), F32),
            pltpu.VMEM((exp_dev, tp_size, n_slot, part), BF16),
            pltpu.VMEM((ep_size, tok_rows, width), BF16),
            pltpu.VMEM((ep_size, tok_rows, width), BF16),
            dma, dma((exp_dev,)), dma((exp_dev,)), dma((exp_dev,)),
            dma((ep_size,)), dma((ep_size,)),
            dma((CHUNKS, ep_size)), dma((CHUNKS, ep_size)), dma((CHUNKS, ep_size)), dma((CHUNKS, ep_size)),
            dma((exp_dev, chips)), dma((exp_dev, chips)), dma((exp_dev, chips)), dma((exp_dev, chips)),
            dma((ep_size,)), dma((ep_size,)),
        ],
        compiler_params=pltpu.CompilerParams(collective_id=0, has_side_effects=True),
    )(
        tokens, norm_gain.reshape(1, depth), group_ids.T, local_ids.T, group_gate.reshape(1, tok_rows),
        expert_gate.T, lengths.reshape(1, -1), w_gate, w_up, w_down,
    )


def solution(mesh):
    in_specs = (
        P("ep", None),
        P(),
        P("ep", None),
        P("ep", None),
        P("ep"),
        P("ep", None),
        P("ep"),
        P("ep", "tp", None),
        P("ep", "tp", None),
        P("ep", None, "tp"),
    )
    body = functools.partial(local, mesh.shape["ep"], mesh.shape["tp"])
    return jax.shard_map(body, mesh=mesh, in_specs=in_specs, out_specs=P("ep", "tp"), check_vma=False)
```

time: 81.4 us -> 34.3 us (0.42)
  blocking collectives: 35.2 us -> 0 us
  Pallas kernels: 0 us -> 32.6 us
  waiting for transfers between devices: 14.7 us -> 0 us
  between operations: 13.6 us -> 0.01 us
  matrix products: 12.1 us -> 0 us
  other arithmetic: 4.48 us -> 0 us
    all_to_all x3 -> x0, blocking collectives: 35.2 us -> none  [the longest x1 19.4 us: local(): lax.all_to_all(send_rows, 'ep', split_axis=0, concat_axis=0, tiled=True)]
    pallas_call x0 -> x1, Pallas kernels: none -> 32.6 us  [local(): pl.pallas_call(functools.partial(kernel, ep_size, tp_size), out_shape=jax...]
    all_gather x1 -> x0, waiting for transfers between devices: 14.7 us -> none  [local(): lax.all_gather(hidden, 'tp', axis=2, tiled=True)]
    dot_general x7 -> x0, matrix products: 12.1 us -> none  [the longest x1 3.23 us: local(): jnp.einsum('ref,efd->red', lax.all_gather(hidden, 'tp', axis=2, tiled=Tru...]
    reduce_sum x4 -> x0, other arithmetic: 2.12 us -> none  [the longest x1 1.11 us: norm_rows(): scale = lax.rsqrt(jnp.mean(values * values, axis=1, keepdims=True) + 1e-06)]
    convert_element_type x3 -> x0, other arithmetic: 1.46 us -> none  [the longest x1 0.73 us: local(): member_int = (group_ids == group_cols[None, :]).astype(jnp.int32)]
    unnamed x14 -> x1, local copies, waits for them, and re-layouts: 0.21 us -> 1.38 us
  transfers between devices with their start and end apart: 1 -> 0, of which waited for: 1 -> 0; matrix products, arithmetic and copies ran while one was open for 2% -> 0% of each run, Pallas kernels for 0% -> 0%
where the time goes in v1:
time: 34.3 us; the launch traced here: 34 us
  Pallas kernels  32.6 us (95%)
  local copies, waits for them, and re-layouts  1.38 us (4%)
    pallas_call x1, Pallas kernels, local(): pl.pallas_call(functools.partial(kernel, ep_size, tp_size), out_shape=jax...  32.6 us
    unnamed x1, local copies, waits for them, and re-layouts  1.38 us

profile of v1, /device:TPU:0, one launch (start us, length us, event | category | flops | bytes accessed | tf_op | source)
XLA Modules:
  0.0 34.0 jit_solution(14615506808082780501)
XLA Ops:
  0.0 32.6 %shard_map.100 = bf16[32,512]{1,0:T(8,128)(2,1)} custom-call(bf16[32,4096]{1,0:T(8,128)(2,1)} %tokens_hbm.1, f32[1,4096]{1,0:T(1,128)} %bitcast.6, s32[1,32]{1,0:T(1,128)} %bitcast.9, s32[4,32]{1,0:T(4,128)} %bitcast.7, f32[1,32]{1,0:T(1,128)} %bitcast.10, f32[4,32]{1,0:T(4,128)} %bitcast.8, s32[1,8]{1,0:T(1,128)} %bitcast.11, bf16[4,128,4096]{2,1,0:T(8,128)(2,1)} %wg_hbm.1, ...), custom_call_target="tpu_custom_call" | custom-call | tf_op jit(solution)/shard_map/pallas_call | solution.py:236
  32.7 1.4 %copy.12 = bf16[32,512]{1,0:T(8,128)(2,1)} copy(bf16[32,512]{1,0:T(8,128)(2,1)} %shard_map.100) | data formatting | bytes 65536

commit v2 on v1

--- a/solution.py
+++ b/solution.py
@@ -45,10 +45,10 @@
 
 def kernel(
     ep_size, tp_size,
-    tokens_hbm, gain_ref, group_ref, local_ref, group_gate_ref, expert_gate_ref, lengths_ref, wg_hbm, wu_hbm, wd_hbm,
+    tokens_hbm, gain_hbm, group_hbm, local_hbm, group_gate_hbm, expert_gate_hbm, lengths_hbm, wg_hbm, wu_hbm, wd_hbm,
     out_ref,
-    tok, x_all, table_ref, meta, wgu, wd, acc, hid, y_send, y_recv,
-    tok_sem, wg_sem, wu_sem, wd_sem,
+    tok, gain_ref, group_ref, local_ref, group_gate_ref, expert_gate_ref, lengths_ref, x_all, table_ref, meta, wgu, wd, acc, hid, y_send, y_recv,
+    tok_sem, small_sem, wg_sem, wu_sem, wd_sem,
     meta_send, meta_recv, row_send, row_recv, rowf_send, rowf_recv,
     hid_send, hid_recv, hidp_send, hidp_recv, back_send, back_recv,
 ):
@@ -79,27 +79,37 @@
 
     tok_copy = pltpu.make_async_copy(tokens_hbm, tok, tok_sem)
     tok_copy.start()
+    small = [
+        pltpu.make_async_copy(src, dst, small_sem.at[n])
+        for n, (src, dst) in enumerate([
+            (group_hbm, group_ref), (local_hbm, local_ref), (group_gate_hbm, group_gate_ref),
+            (expert_gate_hbm, expert_gate_ref), (lengths_hbm, lengths_ref), (gain_hbm, gain_ref),
+        ])
+    ]
+    for copy in small:
+        copy.start()
+    barrier = pltpu.get_barrier_semaphore()
+    for off in range(1, ep_size):
+        pl.semaphore_signal(barrier, inc=1, device_id=(ep_at(off), tp), device_id_type=MESH)
+    for off in range(1, chips):
+        pl.semaphore_signal(barrier, inc=1, device_id=(ep, tp_at(off)), device_id_type=MESH)
+    pl.semaphore_signal(barrier, inc=1, device_id=(ep, partner), device_id_type=MESH)
+
     wg_copies, wu_copies, wd_copies = [], [], []
     for e in range(exp_dev):
         wg_copies.append(pltpu.make_async_copy(wg_hbm.at[e], wgu.at[e, pl.ds(0, part)], wg_sem.at[e]))
         wu_copies.append(pltpu.make_async_copy(wu_hbm.at[e], wgu.at[e, pl.ds(part, part)], wu_sem.at[e]))
         wd_copies.append(pltpu.make_async_copy(wd_hbm.at[e], wd.at[e], wd_sem.at[e]))
-    for copy in wg_copies + wu_copies + wd_copies:
-        copy.start()
-
-    barrier = pltpu.get_barrier_semaphore()
-    for off in range(1, ep_size):
-        pl.semaphore_signal(barrier, inc=1, device_id=(ep_at(off), tp), device_id_type=MESH)
-    for off in range(1, chips):
-        pl.semaphore_signal(barrier, inc=1, device_id=(ep, tp_at(off)), device_id_type=MESH)
-    pl.semaphore_signal(barrier, inc=1, device_id=(ep, partner), device_id_type=MESH)
-
+    for copy in small:
+        copy.wait()
     tables = token_table(
         group_ref[...], local_ref[...], group_gate_ref[...], expert_gate_ref[...], lengths_ref[...], ep_size, exp_dev
     )
     for i in range(ep_size):
         table_ref[i] = tables[i]
     tok_copy.wait()
+    for copy in wg_copies + wu_copies + wd_copies:
+        copy.start()
     values = tok[...].astype(F32)
     scale = lax.rsqrt(jnp.mean(values * values, axis=1, keepdims=True) + 1e-06)
     x_all[ep] = (values * scale * gain_ref[...]).astype(BF16)
@@ -236,10 +246,16 @@
     return pl.pallas_call(
         functools.partial(kernel, ep_size, tp_size),
         out_shape=jax.ShapeDtypeStruct((tok_rows, width), BF16),
-        in_specs=[anywhere, vmem, vmem, vmem, vmem, vmem, vmem, anywhere, anywhere, anywhere],
+        in_specs=[anywhere] * 10,
         out_specs=vmem,
         scratch_shapes=[
             pltpu.VMEM((tok_rows, depth), BF16),
+            pltpu.VMEM((1, depth), F32),
+            pltpu.VMEM((1, tok_rows), jnp.int32),
+            pltpu.VMEM((local_ids.shape[1], tok_rows), jnp.int32),
+            pltpu.VMEM((1, tok_rows), F32),
+            pltpu.VMEM((local_ids.shape[1], tok_rows), F32),
+            pltpu.VMEM((1, lengths.shape[0]), jnp.int32),
             pltpu.VMEM((ep_size, tok_rows, depth), BF16),
             pltpu.VMEM((ep_size, rows, tok_rows), F32),
             pltpu.VMEM((ep_size, rows, tok_rows), F32),
@@ -249,7 +265,7 @@
             pltpu.VMEM((exp_dev, tp_size, n_slot, part), BF16),
             pltpu.VMEM((ep_size, tok_rows, width), BF16),
             pltpu.VMEM((ep_size, tok_rows, width), BF16),
-            dma, dma((exp_dev,)), dma((exp_dev,)), dma((exp_dev,)),
+            dma, dma((6,)), dma((exp_dev,)), dma((exp_dev,)), dma((exp_dev,)),
             dma((ep_size,)), dma((ep_size,)),
             dma((CHUNKS, ep_size)), dma((CHUNKS, ep_size)), dma((CHUNKS, ep_size)), dma((CHUNKS, ep_size)),
             dma((exp_dev, chips)), dma((exp_dev, chips)), dma((exp_dev, chips)), dma((exp_dev, chips)),

time: 34.3 us -> 31.1 us (0.907)
  Pallas kernels: 32.6 us -> 29.5 us
    pallas_call x1, Pallas kernels: 32.6 us -> 29.5 us  [local(): pl.pallas_call(functools.partial(kernel, ep_size, tp_size), out_shape=jax...]
where the time goes in v2:
time: 31.1 us; the launch traced here: 30.9 us
  Pallas kernels  29.5 us (95%)
  local copies, waits for them, and re-layouts  1.38 us (4%)
    pallas_call x1, Pallas kernels, local(): pl.pallas_call(functools.partial(kernel, ep_size, tp_size), out_shape=jax...  29.5 us
    unnamed x1, local copies, waits for them, and re-layouts  1.38 us

profile of v2, /device:TPU:0, one launch (start us, length us, event | category | flops | bytes accessed | tf_op | source)
XLA Modules:
  0.0 30.9 jit_solution(15432224058663209134)
XLA Ops:
  0.0 29.5 %shard_map.100 = bf16[32,512]{1,0:T(8,128)(2,1)} custom-call(bf16[32,4096]{1,0:T(8,128)(2,1)} %tokens_hbm.1, f32[1,4096]{1,0:T(1,128)} %bitcast.6, s32[1,32]{1,0:T(1,128)} %bitcast.9, s32[4,32]{1,0:T(4,128)} %bitcast.7, f32[1,32]{1,0:T(1,128)} %bitcast.10, f32[4,32]{1,0:T(4,128)} %bitcast.8, s32[1,8]{1,0:T(1,128)} %bitcast.11, bf16[4,128,4096]{2,1,0:T(8,128)(2,1)} %wg_hbm.1, ...), custom_call_target="tpu_custom_call" | custom-call | tf_op jit(solution)/shard_map/pallas_call | solution.py:246
  29.5 1.4 %copy.12 = bf16[32,512]{1,0:T(8,128)(2,1)} copy(bf16[32,512]{1,0:T(8,128)(2,1)} %shard_map.100) | data formatting | bytes 65536
